TPU v7x, 512 devices: a whole 4x4x16 slice. The times are simulated.
512 devices in a mesh: ep: 32 (over z, core), tp: 16 (over y, x).
Axes of the slice: x: 4, y: 4, z: 16, core: 2. Of those that a mesh axis runs over, the one named last changes fastest.
Arguments:
- conv_input: bfloat16 [1024, 65536], P('tp', 'ep'), may hold values from -6 to 6
- out_gate: bfloat16 [1024, 65536], P('tp', 'ep'), may hold values from -6 to 6
- in_gate: bfloat16 [1024, 65536], P('tp', 'ep'), may hold values from -6 to 6
- conv_taps: float32 [3, 1024], replicated, may hold values from -3.5 to 3.5
- mixer_proj: bfloat16 [1024, 2048], P(None, 'tp'), may hold values from -0.1875 to 0.1875
- token_rows: bfloat16 [8192, 2048], P('ep', 'tp'), may hold values from -4000 to 4000
- routes: int32 [8192, 2], P('ep'), may hold values from 0 to 31, as said below
- route_weights: float32 [8192, 2], P('ep'), may hold values from 0.3 to 1
- expert_gate: bfloat16 [32, 2048, 4096], P('ep', None, 'tp'), may hold values from -0.125 to 0.125
- expert_up: bfloat16 [32, 2048, 4096], P('ep', None, 'tp'), may hold values from -0.125 to 0.125
- expert_down: bfloat16 [32, 4096, 2048], P('ep', 'tp'), may hold values from -0.125 to 0.125
Outputs:
- mixed_out: bfloat16 [65536, 2048], P('ep', 'tp')
- expert_out: bfloat16 [8192, 2048], P('ep', 'tp')
Inputs may be any that keep to these rules, and one draw needn't show every extreme that they name: `routes`: in each aligned block of 256 rows, no expert is named more than 32 times and one expert, the same in every block, exactly 32 times; the two experts of a row differ.
All inputs are finite; a program needn't handle non-finite values.
Results may differ from a plain program's by a relative error of at most 0.015.
Values may be sent and summed in bfloat16 or wider, within the bound.
A program may use at most 64 MiB of HBM per device.

v0:
```python
import jax
import jax.numpy as jnp
from jax import lax
from jax.sharding import PartitionSpec as P

KERNEL = 3
EPSILON = 1e-06


def passed_along(value, axis, by):
    devices = lax.axis_size(axis)
    pairs = [(i, i + by) for i in range(devices) if 0 <= i + by < devices]
    return lax.ppermute(value, axis, pairs)


def split_up(value, dim, devices):
    before, after = (value.shape[:dim], value.shape[dim + 1 :])
    return jnp.moveaxis(value.reshape(*before, devices, -1, *after), dim, 0)


def sent_and_summed(value, axis, dim):
    blocks = split_up(value, dim, lax.axis_size(axis))
    arrived = lax.all_to_all(blocks, axis, split_axis=0, concat_axis=0, tiled=True)
    return arrived.astype(jnp.float32).sum(axis=0)


def slot_places(route_ids, capacity, experts):
    flat_ids = route_ids.reshape(-1)
    hit_table = (flat_ids[:, None] == jnp.arange(experts, dtype=jnp.int32)[None, :]).astype(
        jnp.int32
    )
    earlier = jnp.cumsum(hit_table, axis=0) - hit_table
    slot_rank = jnp.sum(earlier * hit_table, axis=1)
    return flat_ids * capacity + slot_rank


def body(
    conv_input,
    out_gate,
    in_gate,
    conv_taps,
    mixer_proj,
    token_rows,
    routes,
    route_weights,
    expert_gate,
    expert_up,
    expert_down,
):
    width_part = conv_input.shape[0]
    length = conv_input.shape[1]
    offset = lax.axis_index("tp") * width_part
    local_taps = lax.dynamic_slice_in_dim(conv_taps, offset, width_part, 1)
    z_rows = (conv_input.astype(jnp.float32) * in_gate.astype(jnp.float32)).astype(jnp.bfloat16)
    rim_rows = passed_along(z_rows[:, length - (KERNEL - 1) :], "ep", 1)
    longer = jnp.concatenate([rim_rows, z_rows], axis=1).astype(jnp.float32)
    conv_sum = jnp.zeros(z_rows.shape, jnp.float32)
    for lag_index in range(KERNEL):
        begin = KERNEL - 1 - lag_index
        conv_sum = conv_sum + local_taps[lag_index][:, None] * longer[:, begin : begin + length]
    gated = (out_gate.astype(jnp.float32) * conv_sum).astype(jnp.bfloat16)
    mixed_sum = lax.dot_general(
        lax.all_gather(gated, "tp", axis=0, tiled=True),
        mixer_proj,
        (((0,), (0,)), ((), ())),
        preferred_element_type=jnp.float32,
    )
    mixed_out = mixed_sum.astype(jnp.bfloat16)
    experts = lax.axis_size("ep")
    rows_b = token_rows.shape[0]
    cols_part = token_rows.shape[1]
    capacity = 4 * rows_b // experts
    slot_total = experts * capacity
    places = slot_places(routes, capacity, experts)
    sources = jnp.arange(2 * rows_b, dtype=jnp.int32) // 2
    gate_weight = expert_gate[0]
    up_weight = expert_up[0]
    down_weight = expert_down[0]
    feature_count = cols_part * lax.axis_size("tp")
    buffer = jnp.zeros((slot_total, cols_part), jnp.bfloat16).at[places].set(token_rows[sources])
    arrived = lax.all_to_all(
        buffer.reshape(experts, capacity, cols_part), "ep", split_axis=0, concat_axis=0, tiled=True
    )
    arrived = arrived.reshape(slot_total, cols_part)
    part_in = lax.all_gather(arrived, "tp", axis=1, tiled=True)
    gate_sum = jnp.dot(part_in, gate_weight, preferred_element_type=jnp.float32)
    up_sum = jnp.dot(part_in, up_weight, preferred_element_type=jnp.float32)
    squares = jnp.sum(jnp.square(part_in.astype(jnp.float32)), axis=1)
    row_scale = lax.rsqrt(squares / feature_count + EPSILON)[:, None]
    hidden = (jax.nn.silu(row_scale * gate_sum) * (row_scale * up_sum)).astype(jnp.bfloat16)
    summed = sent_and_summed(
        lax.dot_general(
            down_weight, hidden, (((0,), (1,)), ((), ())), preferred_element_type=jnp.float32
        ).astype(jnp.bfloat16),
        "tp",
        0,
    )
    expert_rows = summed.astype(jnp.bfloat16).reshape(cols_part, experts, capacity)
    returned = lax.all_to_all(expert_rows, "ep", split_axis=1, concat_axis=1, tiled=True).reshape(
        cols_part, slot_total
    )
    picked = returned[:, places].astype(jnp.float32).reshape(cols_part, rows_b, 2)
    combined = jnp.sum(picked * route_weights[None, :, :], axis=2)
    expert_out = combined.T.astype(jnp.bfloat16)
    return (mixed_out, expert_out)


def solution(mesh):
    return jax.shard_map(
        body,
        mesh=mesh,
        in_specs=(
            P("tp", "ep"),
            P("tp", "ep"),
            P("tp", "ep"),
            P(),
            P(None, "tp"),
            P("ep", "tp"),
            P("ep", None),
            P("ep", None),
            P("ep", None, "tp"),
            P("ep", None, "tp"),
            P("ep", "tp", None),
        ),
        out_specs=(P("ep", "tp"), P("ep", "tp")),
        check_vma=False,
    )
```

profile of v0, /device:TPU:1, one launch (start us, length us, event | category | flops | bytes accessed | tf_op | source)
XLA Modules:
  0.0 242.8 jit_solution(143505425020026601)
XLA Ops:
  7.2 0.0 copy-start
  7.2 0.0 all-gather.5.cloned.1.call-start
  7.2 0.9 copy.26
  8.1 0.1 eq.29
  8.3 0.1 eq.25
  8.4 0.7 broadcast_multiply_fusion
  9.1 1.2 reduce-window.6
  10.3 0.2 slice_reduce_fusion
  10.6 0.1 copy.25
  10.7 0.1 mul.101
  10.9 0.1 fusion.18
  11.0 4.9 %scatter_custom_fusion = bf16[1024,128]{1,0:T(8,128)(2,1)S(1)} fusion(s32[512]{0:T(512)S(1)} %bitcast.65, bf16[256,128]{1,0:T(8,128)(2,1)} %param.16, s32[1024]{0:T(1024)S(1)} %pad_clamp_fusion.1, bf16[]{:T(256)} %constant.39.clone.1), kind=kCustom, calls=%fused_computation.26 | custom fusion | bytes 262656 | tf_op jit(solution)/shard_map/scatter | solution.py:80
  15.9 38.9 %all_to_all.15 = bf16[32,32,128]{2,1,0:T(8,128)(2,1)} all-to-all(bf16[32,32,128]{2,1,0:T(8,128)(2,1)S(1)} %bitcast.63), channel_id=1, replica_groups=mesh['ep'=32,'tp'=16] {'ep'}, dimensions={0} | all-to-all | bytes 524288 | tf_op jit(solution)/shard_map/all_to_all | solution.py:81
  54.8 0.0 copy-start.3
  54.8 0.0 all-gather.5.cloned.1.call-update
  54.8 0.0 all-gather.3.cloned.1.call-start
  54.9 1.2 multiply_convert_fusion
  56.0 0.1 slice.40
  56.1 2.2 collective-permute-start
  58.4 0.8 constant_dynamic-slice_fusion
  59.1 0.1 collective-permute-done
  59.2 0.1 maximum_convert_fusion
  59.4 2.0 fusion.9
  61.4 0.0 all-gather.3.cloned.1.call-update
  61.4 55.6 %all-gather.5.cloned.1.call-done = bf16[1024,2048]{1,0:T(8,128)(2,1)} async-done(((bf16[1024,128]{1,0:T(8,128)(2,1)}), bf16[1024,2048]{1,0:T(8,128)(2,1)}) %all-gather.5.cloned.1.call-update) | async-done | bytes 4194320 | tf_op jit(solution)/shard_map/all_gather | solution.py:85
  117.1 0.0 copy-start.1
  117.1 3.2 %multiply_reduce_fusion = f32[1024]{0:T(1024)S(1)} fusion(bf16[1024,2048]{1,0:T(8,128)(2,1)} %all-gather.5.cloned.1.call-done), kind=kLoop, calls=%fused_computation.3 | loop fusion | flops 6290432 | bytes 4198400 | tf_op jit(solution)/shard_map/reduce_sum | solution.py:88
  120.3 0.0 copy-start.4
  120.3 0.0 copy-done.3
  120.3 0.2 copy-done.1
  120.5 2.3 convolution_multiply_fusion.1
  122.8 0.0 copy-done
  122.8 0.0 copy-done.4
  122.8 8.8 %convert_bitcast_fusion = bf16[128,16,8,128]{3,2,1,0:T(8,128)(2,1)} fusion(bf16[1,256,2048]{2,1,0:T(8,128)(2,1)S(1)} %copy-done, bf16[1024,2048]{1,0:T(8,128)(2,1)} %all-gather.5.cloned.1.call-done, bf16[1,2048,256]{2,1,0:T(8,128)(2,1)S(1)} %copy-done.4, f32[1024,256]{1,0:T(8,128)} %convolution_multiply_fusion.1, f32[1024]{0:T(1024)S(1)} %add_rsqrt_fusion), kind=kOutput, calls=%fused_computation.5 | convolution fusion | flops 2151415808 | bytes 11538432 | tf_op jit(solution)/shard_map/dot_general | solution.py:92
  131.6 3.3 %copy.35 = bf16[128,16,8,128]{3,2,0,1:T(8,128)(2,1)S(1)} copy(bf16[128,16,8,128]{3,2,1,0:T(8,128)(2,1)} %convert_bitcast_fusion) | data formatting | bytes 8388608 | tf_op jit(solution)/shard_map/reshape | solution.py:18
  134.9 58.8 %all_to_all.16 = bf16[16,128,1024]{1,2,0:T(8,128)(2,1)} all-to-all(bf16[16,128,1024]{1,2,0:T(8,128)(2,1)S(1)} %bitcast.59), channel_id=1, replica_groups=mesh['ep'=32,'tp'=16] {'tp'}, dimensions={0} | all-to-all | bytes 8388608 | tf_op jit(solution)/shard_map/all_to_all | solution.py:23
  193.7 0.0 copy-start.2
  193.7 0.0 copy-start.5
  193.7 3.9 %reduce_sum.44 = bf16[128,1024]{0,1:T(8,128)(2,1)} reduce(bf16[16,128,1024]{1,2,0:T(8,128)(2,1)} %all_to_all.16, bf16[]{:T(256)} %constant.39.clone.1), dimensions={0}, to_apply=%region_5.6 | reduce | flops 1966080 | bytes 4456450 | tf_op jit(solution)/shard_map/reduce_sum | solution.py:24
  197.6 13.7 %all-to-all-start.2 = ((bf16[128,32,32]{0,2,1:T(8,128)(2,1)}), bf16[128,32,32]{0,2,1:T(8,128)(2,1)S(1)}, u32[]{:S(2)}, u32[]{:S(2)}) async-start(bf16[128,32,32]{0,2,1:T(8,128)(2,1)} %bitcast.13), calls=%async_computation.2 | async-start | bytes 524288 | tf_op jit(solution)/shard_map/all_to_all | solution.py:99
  211.3 0.0 copy-done.2
  211.3 0.1 copy.30
  211.5 3.2 %all-gather.3.cloned.1.call-done = bf16[1024,2048]{1,0:T(8,128)(2,1)} async-done(((bf16[64,2048]{1,0:T(8,128)(2,1)}), bf16[1024,2048]{1,0:T(8,128)(2,1)}) %all-gather.3.cloned.1.call-update) | async-done | bytes 4194320 | tf_op jit(solution)/shard_map/all_gather | solution.py:63
  214.7 0.0 copy-done.5
  214.7 4.3 %convolution_convert_fusion = bf16[2048,128]{1,0:T(8,128)(2,1)} fusion(bf16[1024,2048]{1,0:T(8,128)(2,1)} %all-gather.3.cloned.1.call-done, bf16[1024,128]{1,0:T(8,128)(2,1)S(1)} %copy-done.5), kind=kOutput, calls=%fused_computation.6 | convolution fusion | flops 537133056 | bytes 4980736 | tf_op jit(solution)/shard_map/dot_general | solution.py:62
  219.0 14.6 %all-to-all-done.2 = bf16[128,32,32]{0,2,1:T(8,128)(2,1)S(1)} async-done(((bf16[128,32,32]{0,2,1:T(8,128)(2,1)}), bf16[128,32,32]{0,2,1:T(8,128)(2,1)S(1)}, u32[]{:S(2)}, u32[]{:S(2)}) %all-to-all-start.2) | async-done | bytes 262176 | tf_op jit(solution)/shard_map/all_to_all | solution.py:99
  233.6 1.3 gather_fusion
  234.9 1.0 multiply_reduce_fusion.1
  (10 shorter events, 0.1 us)
Async XLA Ops:
  7.2 115.7 %copy-start = (bf16[1,256,2048]{2,1,0:T(8,128)(2,1)S(1)}, bf16[1,256,2048]{2,1,0:T(8,128)(2,1)}, u32[]{:S(2)}) copy-start(bf16[1,256,2048]{2,1,0:T(8,128)(2,1)} %param.21) | copy-start | bytes 3145732
  7.2 109.9 %all-gather.5.cloned.1.call-start = ((), (), s32[]{:S(2)}) async-start(), calls=%async_computation.4 | async-start | bytes 4456448 | tf_op jit(solution)/shard_map/all_gather | solution.py:85
  54.8 65.5 %copy-start.3 = (bf16[1,2048,256]{2,1,0:T(8,128)(2,1)S(1)}, bf16[1,2048,256]{2,1,0:T(8,128)(2,1)}, u32[]{:S(2)}) copy-start(bf16[1,2048,256]{2,1,0:T(8,128)(2,1)} %param.19) | copy-start | bytes 3145732
  54.8 159.8 %all-gather.3.cloned.1.call-start = ((), (), s32[]{:S(2)}) async-start(), calls=%async_computation.3 | async-start | bytes 4456448 | tf_op jit(solution)/shard_map/all_gather | solution.py:63
  56.1 3.1 %collective-permute-start = (bf16[64,2]{1,0:T(8,128)(2,1)S(1)}, bf16[64,2]{1,0:T(8,128)(2,1)S(1)}, u32[]{:S(2)}, u32[]{:S(2)}) collective-permute-start(bf16[64,2]{1,0:T(8,128)(2,1)S(1)} %slice.40), channel_id=1, source_target_pairs={{0,16},{16,32},{32,48},{48,64},{64,80},{80,96},{96,112},{112,128},... | collective-permute-start | bytes 776 | tf_op jit(solution)/shard_map/ppermute | solution.py:13
  117.1 3.4 %copy-start.1 = (bf16[1024,2048]{1,0:T(8,128)(2,1)S(1)}, bf16[1024,2048]{1,0:T(8,128)(2,1)}, u32[]{:S(2)}) copy-start(bf16[1024,2048]{1,0:T(8,128)(2,1)} %all-gather.5.cloned.1.call-done) | copy-start | bytes 12582916
  120.3 2.5 %copy-start.4 = (bf16[1,2048,256]{2,1,0:T(8,128)(2,1)S(1)}, bf16[1,2048,256]{2,1,0:T(8,128)(2,1)}, u32[]{:S(2)}) copy-start(bf16[1,2048,256]{2,1,0:T(8,128)(2,1)} %param.20) | copy-start | bytes 3145732
  193.7 17.6 %copy-start.2 = (f32[256,2]{0,1:T(2,128)S(1)}, f32[256,2]{0,1:T(2,128)}, u32[]{:S(2)}) copy-start(f32[256,2]{0,1:T(2,128)} %param.18) | copy-start | bytes 6148
  193.7 21.0 %copy-start.5 = (bf16[1024,128]{1,0:T(8,128)(2,1)S(1)}, bf16[1024,128]{1,0:T(8,128)(2,1)}, u32[]{:S(2)}) copy-start(bf16[1024,128]{1,0:T(8,128)(2,1)} %param.15) | copy-start | bytes 786436
  197.6 35.9 %all-to-all-start.2 = ((bf16[128,32,32]{0,2,1:T(8,128)(2,1)}), bf16[128,32,32]{0,2,1:T(8,128)(2,1)S(1)}, u32[]{:S(2)}, u32[]{:S(2)}) async-start(bf16[128,32,32]{0,2,1:T(8,128)(2,1)} %bitcast.13), calls=%async_computation.2 | async-start | bytes 524288 | tf_op jit(solution)/shard_map/all_to_all | solution.py:99
Sparse Core Ops, SparseCore 0:
  54.9 62.0 all-gather.4
  120.6 93.9 all-gather.2
where the time goes:
time: 243 us
  blocking collectives  97.7 us (40%)
  waiting for transfers between devices  73.6 us (30%)
  starting transfers between devices  16 us (7%)
  matrix products  15.4 us (6%)
  between operations  14.2 us (6%)
  other arithmetic  13.6 us (6%)
  local copies, waits for them, and re-layouts  12.4 us (5%)
    all_to_all x1, blocking collectives, sent_and_summed(): lax.all_to_all(blocks, axis, split_axis=0, concat_axis=0, tiled=True)  58.8 us
    all_gather x1, waiting for transfers between devices, body(): part_in = lax.all_gather(arrived, 'tp', axis=1, tiled=True)  55.6 us
    all_to_all x1, blocking collectives, body(): lax.all_to_all(buffer.reshape(experts, capacity, cols_part), 'ep', split_...  38.9 us
    all_to_all x1, waiting for transfers between devices, body(): lax.all_to_all(expert_rows, 'ep', split_axis=1, concat_axis=1, tiled=True)  14.6 us
    all_to_all x1, starting transfers between devices, body(): lax.all_to_all(expert_rows, 'ep', split_axis=1, concat_axis=1, tiled=True)  13.7 us
    dot_general x1, matrix products, body(): lax.dot_general(down_weight, hidden, (((0,), (1,)), ((), ())), preferred_...  8.82 us
    scatter x1, local copies, waits for them, and re-layouts, body(): jnp.zeros((slot_total, cols_part), jnp.bfloat16).at[places]  4.9 us
  transfers between devices with their start and end apart: 4, of which 4 were waited for; matrix products, arithmetic and copies ran while one was open for 12% of the time, Pallas kernels for 0%

commit v1 on v0

--- a/solution.py
+++ b/solution.py
@@ -82,7 +82,9 @@
         buffer.reshape(experts, capacity, cols_part), "ep", split_axis=0, concat_axis=0, tiled=True
     )
     arrived = arrived.reshape(slot_total, cols_part)
-    part_in = lax.all_gather(arrived, "tp", axis=1, tiled=True)
+    part_in = jnp.concatenate(
+        lax.all_to_all(jnp.stack([arrived] * lax.axis_size("tp")), "tp", 0, 0), axis=1
+    )
     gate_sum = jnp.dot(part_in, gate_weight, preferred_element_type=jnp.float32)
     up_sum = jnp.dot(part_in, up_weight, preferred_element_type=jnp.float32)
     squares = jnp.sum(jnp.square(part_in.astype(jnp.float32)), axis=1)

time: 243 us -> 251 us (1.033)
  starting transfers between devices: 16 us -> 22.4 us
  blocking collectives: 97.7 us -> 92.7 us
  waiting for transfers between devices: 73.6 us -> 77 us
  matrix products: 15.4 us -> 18 us
    all_to_all x0 -> x1, waiting for transfers between devices: none -> 59.2 us  [body(): lax.all_to_all(jnp.stack([arrived] * lax.axis_size('tp')), 'tp', 0, 0)]
    all_gather x1 -> x0, waiting for transfers between devices: 55.6 us -> none  [body(): part_in = lax.all_gather(arrived, 'tp', axis=1, tiled=True)]
    all_to_all x0 -> x1, starting transfers between devices: none -> 6.94 us  [body(): lax.all_to_all(jnp.stack([arrived] * lax.axis_size('tp')), 'tp', 0, 0)]
    all_to_all x1, blocking collectives: 58.8 us -> 53.9 us  [sent_and_summed(): lax.all_to_all(blocks, axis, split_axis=0, concat_axis=0, tiled=True)]
    all_gather x1, waiting for transfers between devices: 3.18 us -> 0.02 us  [body(): lax.all_gather(gated, 'tp', axis=0, tiled=True)]
    all_to_all x1, waiting for transfers between devices: 14.6 us -> 17.8 us  [body(): lax.all_to_all(expert_rows, 'ep', split_axis=1, concat_axis=1, tiled=True)]
    another operation x1 -> x3, local copies, waits for them, and re-layouts: 0.01 us -> 2.66 us  [the longest x2 2.66 us: body(): jnp.stack([arrived] * lax.axis_size('tp'))]
  transfers between devices with their start and end apart: 4 -> 4, of which waited for: 4 -> 2; matrix products, arithmetic and copies ran while one was open for 12% -> 12% of each run, Pallas kernels for 0% -> 0%
where the time goes in v1:
time: 251 us; the launch traced here: 250 us
  blocking collectives  92.7 us (37%)
  waiting for transfers between devices  77 us (31%)
  starting transfers between devices  22.4 us (9%)
  matrix products  18 us (7%)
  local copies, waits for them, and re-layouts  14.9 us (6%)
  between operations  14.3 us (6%)
  other arithmetic  11.1 us (4%)
    all_to_all x1, waiting for transfers between devices, body(): lax.all_to_all(jnp.stack([arrived] * lax.axis_size('tp')), 'tp', 0, 0)  59.2 us
    all_to_all x1, blocking collectives, sent_and_summed(): lax.all_to_all(blocks, axis, split_axis=0, concat_axis=0, tiled=True)  53.9 us
    all_to_all x1, blocking collectives, body(): lax.all_to_all(buffer.reshape(experts, capacity, cols_part), 'ep', split_...  38.8 us
    all_to_all x1, waiting for transfers between devices, body(): lax.all_to_all(expert_rows, 'ep', split_axis=1, concat_axis=1, tiled=True)  17.8 us
    all_to_all x1, starting transfers between devices, body(): lax.all_to_all(expert_rows, 'ep', split_axis=1, concat_axis=1, tiled=True)  12.6 us
    dot_general x1, matrix products, body(): lax.dot_general(down_weight, hidden, (((0,), (1,)), ((), ())), preferred_...  9.14 us
    all_to_all x1, starting transfers between devices, body(): lax.all_to_all(jnp.stack([arrived] * lax.axis_size('tp')), 'tp', 0, 0)  6.94 us
  transfers between devices with their start and end apart: 4, of which 2 were waited for; matrix products, arithmetic and copies ran while one was open for 12% of the time, Pallas kernels for 0%

profile of v1, /device:TPU:1, one launch (start us, length us, event | category | flops | bytes accessed | tf_op | source)
XLA Modules:
  0.0 250.4 jit_solution(8188873265201765081)
XLA Ops:
  7.2 0.0 copy-start
  7.2 0.9 copy.26
  8.1 0.1 eq.29
  8.2 0.1 eq.25
  8.4 0.7 broadcast_multiply_fusion
  9.1 1.2 reduce-window.6
  10.3 0.2 slice_reduce_fusion
  10.5 0.1 copy.25
  10.7 0.1 mul.101
  10.8 0.1 fusion.18
  10.9 4.9 %scatter_custom_fusion = bf16[1024,128]{1,0:T(8,128)(2,1)S(1)} fusion(s32[512]{0:T(512)S(1)} %bitcast.69, bf16[256,128]{1,0:T(8,128)(2,1)} %param.16, s32[1024]{0:T(1024)S(1)} %pad_clamp_fusion.1, bf16[]{:T(256)} %constant.39.clone.1), kind=kCustom, calls=%fused_computation.26 | custom fusion | bytes 262656 | tf_op jit(solution)/shard_map/scatter | solution.py:80
  15.9 38.8 %all_to_all.20 = bf16[32,32,128]{2,1,0:T(8,128)(2,1)S(1)} all-to-all(bf16[32,32,128]{2,1,0:T(8,128)(2,1)S(1)} %bitcast.66), channel_id=1, replica_groups=mesh['ep'=32,'tp'=16] {'ep'}, dimensions={0} | all-to-all | bytes 524288 | tf_op jit(solution)/shard_map/all_to_all | solution.py:81
  54.6 0.1 copy.29
  54.8 2.5 %stack.3 = bf16[16,1024,128]{1,2,0:T(8,128)(2,1)} broadcast(bf16[1024,128]{0,1:T(8,128)(2,1)S(1)} %copy.29), dimensions={1,2} | broadcast | bytes 4456448 | tf_op jit(solution)/shard_map/stack | solution.py:86
  57.3 0.0 copy-start.1
  57.3 0.0 copy-start.2
  57.3 6.9 %all-to-all-start.1 = ((bf16[16,1024,128]{1,2,0:T(8,128)(2,1)}), bf16[16,1024,128]{1,2,0:T(8,128)(2,1)}, u32[]{:S(2)}, u32[]{:S(2)}) async-start(bf16[16,1024,128]{1,2,0:T(8,128)(2,1)} %stack.3), calls=%async_computation.1 | async-start | bytes 8388608 | tf_op jit(solution)/shard_map/all_to_all | solution.py:86
  64.3 0.0 copy-start.5
  64.3 0.0 all-gather.2.cloned.1.call-start
  64.3 0.0 copy-done.1
  64.3 0.0 copy-done.2
  64.3 0.1 multiply_convert_fusion
  64.4 0.1 slice.40
  64.5 2.8 %collective-permute-start = (bf16[64,2]{1,0:T(8,128)(2,1)S(1)}, bf16[64,2]{1,0:T(8,128)(2,1)S(1)}, u32[]{:S(2)}, u32[]{:S(2)}) collective-permute-start(bf16[64,2]{1,0:T(8,128)(2,1)S(1)} %slice.40), channel_id=1, source_target_pairs={{0,16},{16,32},{32,48},{48,64},{64,80},{80,96},{96,112},{112,128},... | collective-permute-start | bytes 776 | tf_op jit(solution)/shard_map/ppermute | solution.py:13
  67.3 0.8 constant_dynamic-slice_fusion
  68.1 0.0 collective-permute-done
  68.1 0.1 maximum_convert_fusion
  68.3 0.0 copy-done.3
  68.3 1.1 fusion.9
  69.3 0.0 all-gather.2.cloned.1.call-update
  69.4 59.2 %all-to-all-done.1 = bf16[16,1024,128]{1,2,0:T(8,128)(2,1)} async-done(((bf16[16,1024,128]{1,2,0:T(8,128)(2,1)}), bf16[16,1024,128]{1,2,0:T(8,128)(2,1)}, u32[]{:S(2)}, u32[]{:S(2)}) %all-to-all-start.1) | async-done | bytes 4194336 | tf_op jit(solution)/shard_map/all_to_all | solution.py:86
  128.6 3.1 %multiply_reduce_fusion = f32[1024]{0:T(1024)S(1)} fusion(bf16[16,1024,128]{1,2,0:T(8,128)(2,1)} %all-to-all-done.1), kind=kLoop, calls=%fused_computation.3 | loop fusion | flops 6290432 | bytes 4198400 | tf_op jit(solution)/shard_map/reduce_sum | solution.py:90
  131.7 0.0 copy-done.5
  131.7 4.6 %convolution_multiply_fusion.1 = f32[1024,256]{1,0:T(8,128)} fusion(bf16[1024,2048]{0,1:T(8,128)(2,1)} %bitcast.10, bf16[1,2048,256]{2,1,0:T(8,128)(2,1)S(1)} %copy-done.5, f32[1024]{0:T(1024)S(1)} %add_rsqrt_fusion), kind=kOutput, calls=%fused_computation.8 | convolution fusion | flops 1074003968 | bytes 6295552 | tf_op jit(solution)/shard_map/dot_general | solution.py:88
  136.2 0.0 copy-done
  136.2 9.1 %convert_bitcast_fusion = bf16[128,16,8,128]{3,2,1,0:T(8,128)(2,1)} fusion(bf16[1,256,2048]{2,1,0:T(8,128)(2,1)S(1)} %copy-done, bf16[1024,2048]{0,1:T(8,128)(2,1)} %bitcast.10, bf16[1,2048,256]{2,1,0:T(8,128)(2,1)} %param.20, f32[1024,256]{1,0:T(8,128)} %convolution_multiply_fusion.1, f32[1024]{0:T(1024)S(1)} %add_rsqrt_fusion), kind=kOutput, calls=%fused_computation.5 | convolution fusion | flops 2151415808 | bytes 11538432 | tf_op jit(solution)/shard_map/dot_general | solution.py:94
  145.4 3.3 %copy.36 = bf16[128,16,8,128]{3,2,0,1:T(8,128)(2,1)S(1)} copy(bf16[128,16,8,128]{3,2,1,0:T(8,128)(2,1)} %convert_bitcast_fusion) | data formatting | bytes 8388608 | tf_op jit(solution)/shard_map/reshape | solution.py:18
  148.7 53.9 %all_to_all.21 = bf16[16,128,1024]{1,2,0:T(8,128)(2,1)} all-to-all(bf16[16,128,1024]{1,2,0:T(8,128)(2,1)S(1)} %bitcast.63), channel_id=1, replica_groups=mesh['ep'=32,'tp'=16] {'tp'}, dimensions={0} | all-to-all | bytes 8388608 | tf_op jit(solution)/shard_map/all_to_all | solution.py:23
  202.7 3.6 %reduce_sum.44 = bf16[128,1024]{0,1:T(8,128)(2,1)} reduce(bf16[16,128,1024]{1,2,0:T(8,128)(2,1)} %all_to_all.21, bf16[]{:T(256)} %constant.39.clone.1), dimensions={0}, to_apply=%region_5.6 | reduce | flops 1966080 | bytes 4456450 | tf_op jit(solution)/shard_map/reduce_sum | solution.py:24
  206.3 12.6 %all-to-all-start.3 = ((bf16[128,32,32]{0,2,1:T(8,128)(2,1)}), bf16[128,32,32]{0,2,1:T(8,128)(2,1)S(1)}, u32[]{:S(2)}, u32[]{:S(2)}) async-start(bf16[128,32,32]{0,2,1:T(8,128)(2,1)} %bitcast.16), calls=%async_computation.3 | async-start | bytes 524288 | tf_op jit(solution)/shard_map/all_to_all | solution.py:101
  218.9 0.0 copy-done.4
  218.9 0.1 copy.31
  219.1 0.0 all-gather.2.cloned.1.call-done
  219.1 0.0 copy-done.6
  219.1 4.3 %convolution_convert_fusion = bf16[2048,128]{1,0:T(8,128)(2,1)} fusion(bf16[1024,2048]{1,0:T(8,128)(2,1)} %all-gather.2.cloned.1.call-done, bf16[1024,128]{1,0:T(8,128)(2,1)S(1)} %copy-done.6), kind=kOutput, calls=%fused_computation.6 | convolution fusion | flops 537133056 | bytes 4980736 | tf_op jit(solution)/shard_map/dot_general | solution.py:62
  223.4 17.8 %all-to-all-done.3 = bf16[128,32,32]{0,2,1:T(8,128)(2,1)S(1)} async-done(((bf16[128,32,32]{0,2,1:T(8,128)(2,1)}), bf16[128,32,32]{0,2,1:T(8,128)(2,1)S(1)}, u32[]{:S(2)}, u32[]{:S(2)}) %all-to-all-start.3) | async-done | bytes 262176 | tf_op jit(solution)/shard_map/all_to_all | solution.py:101
  241.2 1.3 gather_fusion
  242.5 1.0 multiply_reduce_fusion.1
  (13 shorter events, 0.1 us)
Async XLA Ops:
  7.2 129.1 %copy-start = (bf16[1,256,2048]{2,1,0:T(8,128)(2,1)S(1)}, bf16[1,256,2048]{2,1,0:T(8,128)(2,1)}, u32[]{:S(2)}) copy-start(bf16[1,256,2048]{2,1,0:T(8,128)(2,1)} %param.21) | copy-start | bytes 3145732
  57.3 7.0 %copy-start.1 = (bf16[64,2048]{1,0:T(8,128)(2,1)S(1)}, bf16[64,2048]{1,0:T(8,128)(2,1)}, u32[]{:S(2)}) copy-start(bf16[64,2048]{1,0:T(8,128)(2,1)} %param.13) | copy-start | bytes 786436
  57.3 7.0 %copy-start.2 = (bf16[64,2048]{1,0:T(8,128)(2,1)S(1)}, bf16[64,2048]{1,0:T(8,128)(2,1)}, u32[]{:S(2)}) copy-start(bf16[64,2048]{1,0:T(8,128)(2,1)} %param.11) | copy-start | bytes 786436
  57.3 10.9 %copy-start.3 = (bf16[64,2048]{1,0:T(8,128)(2,1)S(1)}, bf16[64,2048]{1,0:T(8,128)(2,1)}, u32[]{:S(2)}) copy-start(bf16[64,2048]{1,0:T(8,128)(2,1)} %param.12) | copy-start | bytes 786436
  57.3 71.2 %all-to-all-start.1 = ((bf16[16,1024,128]{1,2,0:T(8,128)(2,1)}), bf16[16,1024,128]{1,2,0:T(8,128)(2,1)}, u32[]{:S(2)}, u32[]{:S(2)}) async-start(bf16[16,1024,128]{1,2,0:T(8,128)(2,1)} %stack.3), calls=%async_computation.1 | async-start | bytes 8388608 | tf_op jit(solution)/shard_map/all_to_all | solution.py:86
  64.3 67.4 %copy-start.5 = (bf16[1,2048,256]{2,1,0:T(8,128)(2,1)S(1)}, bf16[1,2048,256]{2,1,0:T(8,128)(2,1)}, u32[]{:S(2)}) copy-start(bf16[1,2048,256]{2,1,0:T(8,128)(2,1)} %param.19) | copy-start | bytes 3145732
  64.3 154.8 %all-gather.2.cloned.1.call-start = ((), (), s32[]{:S(2)}) async-start(), calls=%async_computation.4 | async-start | bytes 4456448 | tf_op jit(solution)/shard_map/all_gather | solution.py:63
  64.5 3.6 %collective-permute-start = (bf16[64,2]{1,0:T(8,128)(2,1)S(1)}, bf16[64,2]{1,0:T(8,128)(2,1)S(1)}, u32[]{:S(2)}, u32[]{:S(2)}) collective-permute-start(bf16[64,2]{1,0:T(8,128)(2,1)S(1)} %slice.40), channel_id=1, source_target_pairs={{0,16},{16,32},{32,48},{48,64},{64,80},{80,96},{96,112},{112,128},... | collective-permute-start | bytes 776 | tf_op jit(solution)/shard_map/ppermute | solution.py:13
  202.7 16.2 %copy-start.4 = (f32[256,2]{0,1:T(2,128)S(1)}, f32[256,2]{0,1:T(2,128)}, u32[]{:S(2)}) copy-start(f32[256,2]{0,1:T(2,128)} %param.18) | copy-start | bytes 6148
  202.7 16.4 %copy-start.6 = (bf16[1024,128]{1,0:T(8,128)(2,1)S(1)}, bf16[1024,128]{1,0:T(8,128)(2,1)}, u32[]{:S(2)}) copy-start(bf16[1024,128]{1,0:T(8,128)(2,1)} %param.15) | copy-start | bytes 786436
  206.3 34.9 %all-to-all-start.3 = ((bf16[128,32,32]{0,2,1:T(8,128)(2,1)}), bf16[128,32,32]{0,2,1:T(8,128)(2,1)S(1)}, u32[]{:S(2)}, u32[]{:S(2)}) async-start(bf16[128,32,32]{0,2,1:T(8,128)(2,1)} %bitcast.16), calls=%async_computation.3 | async-start | bytes 524288 | tf_op jit(solution)/shard_map/all_to_all | solution.py:101
Sparse Core Ops, SparseCore 0:
  69.5 85.3 all-gather.1
